TPU v7x, 256 devices: a whole 4x4x8 slice. The times are simulated.
256 devices in a mesh: ep: 16 (over y, x), tp: 16 (over z, core).
Axes of the slice: x: 4, y: 4, z: 8, core: 2. Of those that a mesh axis runs over, the one named last changes fastest.
Arguments:
- mix_tokens: bfloat16 [32768, 2048], P(('ep', 'tp')), may hold values from -6 to 6
- mix_gain: bfloat16 [2048], replicated, may hold values from 0.099609375 to 1.8984375
- gate_proj: bfloat16 [2048, 1024], P(None, 'tp'), may hold values from -0.125 to 0.125
- conv_proj: bfloat16 [2048, 1024], P(None, 'tp'), may hold values from -0.125 to 0.125
- value_proj: bfloat16 [2048, 1024], P(None, 'tp'), may hold values from -0.125 to 0.125
- conv_taps: bfloat16 [3, 1024], P(None, 'tp'), may hold values from -3 to 3
- out_proj: bfloat16 [1024, 2048], P('tp'), may hold values from -0.1875 to 0.1875
- moe_tokens: bfloat16 [16384, 2048], P(('ep', 'tp')), may hold values from -6 to 6
- moe_gain: bfloat16 [2048], replicated, may hold values from 0.099609375 to 1.8984375
- expert_ids: int32 [16384, 2], P(('ep', 'tp')), may hold values from 0 to 15, all different within a row; in each aligned block of 64 rows (0 to 63, 64 to 127, ...) at most 9 rows name the same one
- expert_scores: float32 [16384, 2], P(('ep', 'tp')), may hold values from -6 to 6
- expert_gate: bfloat16 [16, 2048, 4096], P('ep', None, 'tp'), may hold values from -0.125 to 0.125
- expert_up: bfloat16 [16, 2048, 4096], P('ep', None, 'tp'), may hold values from -0.125 to 0.125
- expert_down: bfloat16 [16, 4096, 2048], P('ep', 'tp'), may hold values from -0.09375 to 0.09375
Outputs:
- mix_out: bfloat16 [32768, 2048], P(('ep', 'tp'))
- moe_out: bfloat16 [16384, 2048], P(('ep', 'tp'))
Inputs may be any that keep to these rules, and one draw needn't show every extreme that they name: `expert_ids`: each row names 2 different experts; among the rows of one device no expert is named more than 9 times.
All inputs are finite; a program needn't handle non-finite values.
Results may differ from a plain program's by a relative error of at most 0.018.
Values may be sent and summed in bfloat16 or wider, within the bound.
A program may use at most 128 MiB of HBM per device.

v0:
```python
import jax
import jax.numpy as jnp
from jax import lax
from jax.sharding import PartitionSpec as P

norm_eps = 1e-06


def from_behind(value, axis, steps):
    count = lax.axis_size(axis)
    leading, last = (max(0, -steps), min(count, count - steps))
    return lax.ppermute(value, axis, [(source, source + steps) for source in range(leading, last)])


def scaled_norm(row_data, gain_vec):
    values = row_data.astype(jnp.float32)
    inverse = lax.rsqrt(jnp.mean(values * values, axis=1, keepdims=True) + norm_eps)
    return (values * inverse * gain_vec.astype(jnp.float32)).astype(jnp.bfloat16)


def shards(
    mix_tokens,
    mix_gain,
    gate_proj,
    conv_proj,
    value_proj,
    conv_taps,
    out_proj,
    moe_tokens,
    moe_gain,
    expert_ids,
    expert_scores,
    expert_gate,
    expert_up,
    expert_down,
):
    normed = scaled_norm(mix_tokens, mix_gain)
    w_joint = jnp.concatenate([gate_proj, conv_proj, value_proj], axis=1)
    combined = jnp.dot(
        lax.all_gather(normed, "tp", axis=0, tiled=True),
        w_joint,
        preferred_element_type=jnp.float32,
    ).astype(jnp.bfloat16)
    channels = gate_proj.shape[1]
    out_gate = combined[:, :channels]
    in_gate = combined[:, channels : 2 * channels]
    values = combined[:, 2 * channels :]
    signal = (in_gate.astype(jnp.float32) * values.astype(jnp.float32)).astype(jnp.bfloat16)
    tap_count = conv_taps.shape[0]
    before = from_behind(signal[signal.shape[0] - (tap_count - 1) :], "ep", 1)
    extended = jnp.concatenate([before, signal], axis=0)
    length = signal.shape[0]
    tap_values = conv_taps.astype(jnp.float32)
    convolved = jnp.zeros((length, channels), jnp.float32)
    for offset in range(tap_count):
        convolved = (
            convolved + extended[offset : offset + length].astype(jnp.float32) * tap_values[offset]
        )
    carried = (out_gate.astype(jnp.float32) * convolved).astype(jnp.bfloat16)
    token_major = lax.all_to_all(carried, "tp", split_axis=0, concat_axis=1, tiled=True)
    mix_out = jnp.dot(
        token_major,
        lax.all_gather(out_proj, "tp", axis=0, tiled=True),
        preferred_element_type=jnp.float32,
    ).astype(jnp.bfloat16)
    moe_normed = scaled_norm(moe_tokens, moe_gain)
    experts = expert_gate.shape[0] * lax.axis_size("ep")
    row_count, top_count = expert_ids.shape
    capacity = top_count * row_count // experts + max(1, top_count * row_count // (8 * experts))
    width_model = moe_tokens.shape[1]
    flat_ids = expert_ids.reshape(-1)
    onehot = (flat_ids[:, None] == jnp.arange(experts, dtype=jnp.int32)[None, :]).astype(jnp.int32)
    slot_rank = jnp.sum((jnp.cumsum(onehot, axis=0) - onehot) * onehot, axis=1)
    slot_index = flat_ids * capacity + slot_rank
    slot_match = slot_index[:, None] == jnp.arange(experts * capacity, dtype=jnp.int32)[None, :]
    dispatch_map = jnp.any(
        slot_match.reshape(row_count, top_count, experts * capacity), axis=1
    ).astype(jnp.bfloat16)
    outgoing = lax.dot_general(
        dispatch_map, moe_normed, (((0,), (0,)), ((), ())), preferred_element_type=jnp.float32
    ).astype(jnp.bfloat16)
    arrived = lax.all_to_all(
        outgoing.reshape(experts, capacity, width_model),
        "ep",
        split_axis=0,
        concat_axis=0,
        tiled=True,
    )
    arrived_rows = arrived.reshape(-1, width_model)
    w_gate = expert_gate[0]
    w_up = expert_up[0]
    w_down = expert_down[0]
    portion = lax.all_gather(arrived_rows, "tp", axis=0, tiled=True)
    gate_value = jnp.dot(portion, w_gate, preferred_element_type=jnp.float32)
    up_value = jnp.dot(portion, w_up, preferred_element_type=jnp.float32)
    hidden = (jax.nn.silu(gate_value) * up_value).astype(jnp.bfloat16)
    summed = lax.psum_scatter(
        jnp.dot(hidden, w_down, preferred_element_type=jnp.float32).astype(jnp.bfloat16),
        "tp",
        scatter_dimension=0,
        tiled=True,
    )
    returned = lax.all_to_all(
        summed.reshape(experts, capacity, width_model),
        "ep",
        split_axis=0,
        concat_axis=0,
        tiled=True,
    )
    flat_back = returned.reshape(experts * capacity, width_model)
    picked = flat_back[slot_index].reshape(row_count, top_count, width_model)
    route_weight = jax.nn.softmax(expert_scores, axis=1)
    moe_out = jnp.sum(route_weight[:, :, None] * picked.astype(jnp.float32), axis=1).astype(
        jnp.bfloat16
    )
    return (mix_out, moe_out)


def solution(mesh):
    in_specs = (
        P(("ep", "tp"), None),
        P(),
        P(None, "tp"),
        P(None, "tp"),
        P(None, "tp"),
        P(None, "tp"),
        P("tp", None),
        P(("ep", "tp"), None),
        P(),
        P(("ep", "tp"), None),
        P(("ep", "tp"), None),
        P("ep", None, "tp"),
        P("ep", None, "tp"),
        P("ep", "tp", None),
    )
    out_specs = (P(("ep", "tp"), None), P(("ep", "tp"), None))
    return jax.shard_map(shards, mesh=mesh, in_specs=in_specs, out_specs=out_specs, check_vma=False)
```

profile of v0, /device:TPU:1, one launch (start us, length us, event | category | flops | bytes accessed | tf_op | source)
XLA Modules:
  0.0 292.0 jit_solution(8549273080741177627)
XLA Ops:
  7.2 0.0 copy-start
  7.2 0.0 all-gather.8.cloned.1.call-start
  7.2 0.8 copy.25
  8.1 0.1 eq.29
  8.2 0.1 fusion.24
  8.3 0.2 reduce_window_sum.11
  8.5 0.2 select_reduce_fusion
  8.7 0.1 reduce_sum.52
  8.8 0.1 copy.27
  8.9 0.1 fusion.23
  9.0 0.7 convert_element_type.89
  9.7 1.1 fusion.15
  10.8 1.3 convolution_convert_fusion.2
  12.2 0.2 reshape.87
  12.4 23.4 %all_to_all.29 = bf16[16,9,2048]{2,1,0:T(8,128)(2,1)S(1)} all-to-all(bf16[16,9,2048]{2,1,0:T(8,128)(2,1)S(1)} %reshape.87), channel_id=1, replica_groups=mesh['ep'=16,'tp'=16] {'ep'}, dimensions={0} | all-to-all | bytes 1179648 | tf_op jit(solution)/shard_map/all_to_all | solution.py:82
  35.8 1.1 reshape.88
  36.9 0.0 all-gather.8.cloned.1.call-update
  36.9 0.0 all-gather.4.cloned.1.call-start
  37.0 0.2 fusion.2
  37.2 1.0 fusion.4
  38.2 0.0 all-gather.4.cloned.1.call-update
  38.2 0.0 reduce-scatter.2.cloned.1.call-start
  38.3 60.5 %all-gather.8.cloned.1.call-done = bf16[2304,2048]{1,0:T(8,128)(2,1)} async-done(((bf16[144,2048]{1,0:T(8,128)(2,1)}), bf16[2304,2048]{1,0:T(8,128)(2,1)}) %all-gather.8.cloned.1.call-update) | async-done | bytes 9437200 | tf_op jit(solution)/shard_map/all_gather | solution.py:93
  98.7 7.7 %fusion.8 = f32[2304,256]{1,0:T(8,128)} fusion(bf16[2304,2048]{1,0:T(8,128)(2,1)} %all-gather.8.cloned.1.call-done, bf16[1,2048,256]{2,1,0:T(8,128)(2,1)S(1)} %copy-done.5), kind=kOutput, calls=%fused_computation.15 | convolution fusion | flops 2415919104 | bytes 12845056 | tf_op jit(solution)/shard_map/dot_general | solution.py:94
  106.5 14.9 %convolution_convert_fusion = bf16[2304,2048]{1,0:T(8,128)(2,1)} fusion(bf16[2304,2048]{1,0:T(8,128)(2,1)} %all-gather.8.cloned.1.call-done, f32[2304,256]{1,0:T(8,128)} %fusion.8, bf16[1,256,2048]{2,1,0:T(8,128)(2,1)S(1)} %copy-done, bf16[1,2048,256]{2,1,0:T(8,128)(2,1)} %param.26), kind=kOutput, calls=%fused_computation.1 | convolution fusion | flops 4840095744 | bytes 23330816 | tf_op jit(solution)/shard_map/dot_general | solution.py:98
  121.4 0.0 reduce-scatter.2.cloned.1.call-update
  121.4 0.0 all-gather.6.cloned.1.call-start
  121.5 0.5 all-gather.6.cloned.1.call-update
  122.0 0.1 copy-done.4
  122.1 33.5 %all-gather.4.cloned.1.call-done = bf16[2048,2048]{1,0:T(8,128)(2,1)} async-done(((bf16[128,2048]{1,0:T(8,128)(2,1)}), bf16[2048,2048]{1,0:T(8,128)(2,1)}) %all-gather.4.cloned.1.call-update) | async-done | bytes 8388624 | tf_op jit(solution)/shard_map/all_gather | solution.py:40
  155.6 6.3 %convolution_convert_fusion.1 = bf16[2048,192]{0,1:T(8,128)(2,1)S(1)} fusion(bf16[2048,2048]{1,0:T(8,128)(2,1)} %all-gather.4.cloned.1.call-done, bf16[2048,64]{0,1:T(8,128)(2,1)S(1)} %copy-done.6, bf16[2048,64]{0,1:T(8,128)(2,1)S(1)} %copy-done.7, bf16[2048,64]{0,1:T(8,128)(2,1)S(1)} %copy-done.8), kind=kOutput, calls=%fused_computation.4 | convolution fusion | flops 1613365248 | bytes 9961472 | tf_op jit(solution)/shard_map/dot_general | solution.py:39
  161.9 0.1 multiply_convert_fusion.1
  162.0 0.1 slice.41
  162.0 3.1 %collective-permute-start = (bf16[2,64]{0,1:T(8,128)(2,1)S(1)}, bf16[2,64]{0,1:T(8,128)(2,1)S(1)}, u32[]{:S(2)}, u32[]{:S(2)}) collective-permute-start(bf16[2,64]{0,1:T(8,128)(2,1)S(1)} %slice.41), channel_id=1, source_target_pairs={{0,16},{16,32},{32,48},{48,64},{64,80},{80,96},{96,112},{112,128},... | collective-permute-start | bytes 776 | tf_op jit(solution)/shard_map/ppermute | solution.py:12
  165.1 0.8 collective-permute-done
  166.0 1.0 copy_bitcast_fusion
  167.0 5.4 %all-to-all-start = ((bf16[16,128,64]{1,2,0:T(8,128)(2,1)}), bf16[16,128,64]{1,2,0:T(8,128)(2,1)S(1)}, u32[]{:S(2)}, u32[]{:S(2)}) async-start(bf16[16,128,64]{1,2,0:T(8,128)(2,1)} %copy_bitcast_fusion), calls=%async_computation | async-start | bytes 524288 | tf_op jit(solution)/shard_map/all_to_all | solution.py:60
  172.4 0.1 mul.138
  172.6 58.9 %reduce-scatter.2.cloned.1.call-done = bf16[144,2048]{1,0:T(8,128)(2,1)} async-done(((bf16[2304,2048]{1,0:T(8,128)(2,1)}), bf16[144,2048]{1,0:T(8,128)(2,1)}) %reduce-scatter.2.cloned.1.call-update) | async-done | bytes 589840 | tf_op jit(solution)/shard_map/reduce_scatter | solution.py:97
  231.5 2.3 reshape.89
  233.8 7.2 %all-to-all-start.2 = ((bf16[16,9,2048]{2,1,0:T(8,128)(2,1)}), bf16[16,9,2048]{2,1,0:T(8,128)(2,1)S(1)}, u32[]{:S(2)}, u32[]{:S(2)}) async-start(bf16[16,9,2048]{2,1,0:T(8,128)(2,1)} %reshape.89), calls=%async_computation.3 | async-start | bytes 2097152 | tf_op jit(solution)/shard_map/all_to_all | solution.py:103
  241.0 0.1 copy.24
  241.1 36.6 %all-gather.6.cloned.1.call-done = bf16[1024,2048]{1,0:T(8,128)(2,1)} async-done(((bf16[64,2048]{1,0:T(8,128)(2,1)}), bf16[1024,2048]{1,0:T(8,128)(2,1)}) %all-gather.6.cloned.1.call-update) | async-done | bytes 4194320 | tf_op jit(solution)/shard_map/all_gather | solution.py:63
  277.7 3.7 %convolution_convert_fusion.3 = bf16[128,2048]{1,0:T(8,128)(2,1)} fusion(bf16[128,1024]{0,1:T(8,128)(2,1)S(1)} %bitcast.36, bf16[1024,2048]{1,0:T(8,128)(2,1)} %all-gather.6.cloned.1.call-done), kind=kOutput, calls=%fused_computation.6 | convolution fusion | flops 537133056 | bytes 4980736 | tf_op jit(solution)/shard_map/dot_general | solution.py:61
  281.4 0.3 reshape.90
  281.6 0.9 gather_fusion
  282.6 0.7 reshape.91
  283.2 2.2 multiply_reduce_fusion
  (29 shorter events, 0.1 us)
Async XLA Ops:
  7.2 99.3 %copy-start = (bf16[1,256,2048]{2,1,0:T(8,128)(2,1)S(1)}, bf16[1,256,2048]{2,1,0:T(8,128)(2,1)}, u32[]{:S(2)}) copy-start(bf16[1,256,2048]{2,1,0:T(8,128)(2,1)} %param.27) | copy-start | bytes 3145732
  7.2 91.6 %all-gather.8.cloned.1.call-start = ((), (), s32[]{:S(2)}) async-start(), calls=%async_computation.6 | async-start | bytes 10027008 | tf_op jit(solution)/shard_map/all_gather | solution.py:93
  12.4 24.6 %copy-start.3 = (bf16[2048]{0:T(1024)(128)(2,1)S(1)}, bf16[2048]{0:T(1024)(128)(2,1)}, u32[]{:S(2)}) copy-start(bf16[2048]{0:T(1024)(128)(2,1)} %param.15) | copy-start | bytes 12292
  35.8 1.2 copy-start.1
  36.9 61.8 %copy-start.5 = (bf16[1,2048,256]{2,1,0:T(8,128)(2,1)S(1)}, bf16[1,2048,256]{2,1,0:T(8,128)(2,1)}, u32[]{:S(2)}) copy-start(bf16[1,2048,256]{2,1,0:T(8,128)(2,1)} %param.25) | copy-start | bytes 3145732
  36.9 118.6 %all-gather.4.cloned.1.call-start = ((), (), s32[]{:S(2)}) async-start(), calls=%async_computation.4 | async-start | bytes 8912896 | tf_op jit(solution)/shard_map/all_gather | solution.py:40
  38.2 193.3 %reduce-scatter.2.cloned.1.call-start = ((), (), s32[]{:S(2)}) async-start(), calls=%async_computation.7 | async-start | bytes 10027008 | tf_op jit(solution)/shard_map/reduce_scatter | solution.py:97
  121.4 0.7 copy-start.4
  121.4 34.2 %copy-start.6 = (bf16[2048,64]{0,1:T(8,128)(2,1)S(1)}, bf16[2048,64]{0,1:T(8,128)(2,1)}, u32[]{:S(2)}) copy-start(bf16[2048,64]{0,1:T(8,128)(2,1)} %param.18) | copy-start | bytes 786436
  121.4 34.2 %copy-start.7 = (bf16[2048,64]{0,1:T(8,128)(2,1)S(1)}, bf16[2048,64]{0,1:T(8,128)(2,1)}, u32[]{:S(2)}) copy-start(bf16[2048,64]{0,1:T(8,128)(2,1)} %param.17) | copy-start | bytes 786436
  121.4 34.2 %copy-start.8 = (bf16[2048,64]{0,1:T(8,128)(2,1)S(1)}, bf16[2048,64]{0,1:T(8,128)(2,1)}, u32[]{:S(2)}) copy-start(bf16[2048,64]{0,1:T(8,128)(2,1)} %param.16) | copy-start | bytes 786436
  121.4 156.2 %all-gather.6.cloned.1.call-start = ((), (), s32[]{:S(2)}) async-start(), calls=%async_computation.5 | async-start | bytes 4456448 | tf_op jit(solution)/shard_map/all_gather | solution.py:63
  122.1 50.5 %copy-start.2 = (f32[64,2]{0,1:T(2,128)S(1)}, f32[64,2]{0,1:T(2,128)}, u32[]{:S(2)}) copy-start(f32[64,2]{0,1:T(2,128)} %param.24) | copy-start | bytes 1540
  162.0 3.9 %collective-permute-start = (bf16[2,64]{0,1:T(8,128)(2,1)S(1)}, bf16[2,64]{0,1:T(8,128)(2,1)S(1)}, u32[]{:S(2)}, u32[]{:S(2)}) collective-permute-start(bf16[2,64]{0,1:T(8,128)(2,1)S(1)} %slice.41), channel_id=1, source_target_pairs={{0,16},{16,32},{32,48},{48,64},{64,80},{80,96},{96,112},{112,128},... | collective-permute-start | bytes 776 | tf_op jit(solution)/shard_map/ppermute | solution.py:12
  167.0 66.8 %all-to-all-start = ((bf16[16,128,64]{1,2,0:T(8,128)(2,1)}), bf16[16,128,64]{1,2,0:T(8,128)(2,1)S(1)}, u32[]{:S(2)}, u32[]{:S(2)}) async-start(bf16[16,128,64]{1,2,0:T(8,128)(2,1)} %copy_bitcast_fusion), calls=%async_computation | async-start | bytes 524288 | tf_op jit(solution)/shard_map/all_to_all | solution.py:60
  233.8 47.6 %all-to-all-start.2 = ((bf16[16,9,2048]{2,1,0:T(8,128)(2,1)}), bf16[16,9,2048]{2,1,0:T(8,128)(2,1)S(1)}, u32[]{:S(2)}, u32[]{:S(2)}) async-start(bf16[16,9,2048]{2,1,0:T(8,128)(2,1)} %reshape.89), calls=%async_computation.3 | async-start | bytes 2097152 | tf_op jit(solution)/shard_map/all_to_all | solution.py:103
Sparse Core Ops, SparseCore 0:
  37.0 61.6 all-gather.7
  101.1 54.3 all-gather.3
  158.1 73.3 reduce-scatter.1
  233.2 44.4 all-gather.5
where the time goes:
time: 293 us; the launch traced here: 292 us
  waiting for transfers between devices  191 us (65%)
  matrix products  34 us (12%)
  blocking collectives  23.4 us (8%)
  starting transfers between devices  15.8 us (5%)
  between operations  14 us (5%)
  local copies, waits for them, and re-layouts  7.02 us (2%)
  other arithmetic  6.89 us (2%)
    all_gather x1, waiting for transfers between devices, shards(): portion = lax.all_gather(arrived_rows, 'tp', axis=0, tiled=True)  60.5 us
    reduce_scatter x1, waiting for transfers between devices, shards(): lax.psum_scatter(jnp.dot(hidden, w_down, preferred_element_type=jnp.float...  58.9 us
    all_gather x1, waiting for transfers between devices, shards(): lax.all_gather(out_proj, 'tp', axis=0, tiled=True)  36.6 us
    all_gather x1, waiting for transfers between devices, shards(): lax.all_gather(normed, 'tp', axis=0, tiled=True)  33.5 us
    all_to_all x1, blocking collectives, shards(): lax.all_to_all(outgoing.reshape(experts, capacity, width_model), 'ep', sp...  23.4 us
    dot_general x1, matrix products, shards(): jnp.dot(hidden, w_down, preferred_element_type=jnp.float32)  14.9 us
    dot_general x1, matrix products, shards(): gate_value = jnp.dot(portion, w_gate, preferred_element_type=jnp.float32)  7.71 us
    all_to_all x1, starting transfers between devices, shards(): lax.all_to_all(summed.reshape(experts, capacity, width_model), 'ep', spli...  7.19 us
  transfers between devices with their start and end apart: 7, of which 5 were waited for; matrix products, arithmetic and copies ran while one was open for 13% of the time, Pallas kernels for 0%

commit v1 on v0

--- a/solution.py
+++ b/solution.py
@@ -90,7 +90,9 @@
     w_gate = expert_gate[0]
     w_up = expert_up[0]
     w_down = expert_down[0]
-    portion = lax.all_gather(arrived_rows, "tp", axis=0, tiled=True)
+    portion = jnp.concatenate(
+        lax.all_to_all(jnp.stack([arrived_rows] * lax.axis_size("tp")), "tp", 0, 0), axis=0
+    )
     gate_value = jnp.dot(portion, w_gate, preferred_element_type=jnp.float32)
     up_value = jnp.dot(portion, w_up, preferred_element_type=jnp.float32)
     hidden = (jax.nn.silu(gate_value) * up_value).astype(jnp.bfloat16)

time: 293 us -> 452 us (1.54)
  waiting for transfers between devices: 191 us -> 335 us
  starting transfers between devices: 15.8 us -> 26.8 us
    all_to_all x0 -> x1, waiting for transfers between devices: none -> 244 us  [shards(): lax.all_to_all(jnp.stack([arrived_rows] * lax.axis_size('tp')), 'tp', 0, 0)]
    all_gather x1 -> x0, waiting for transfers between devices: 60.5 us -> none  [shards(): portion = lax.all_gather(arrived_rows, 'tp', axis=0, tiled=True)]
    all_gather x1, waiting for transfers between devices: 33.5 us -> 0.02 us  [shards(): lax.all_gather(normed, 'tp', axis=0, tiled=True)]
    all_to_all x0 -> x1, starting transfers between devices: none -> 10.7 us  [shards(): lax.all_to_all(jnp.stack([arrived_rows] * lax.axis_size('tp')), 'tp', 0, 0)]
    reduce_scatter x1, waiting for transfers between devices: 58.9 us -> 52.8 us  [shards(): lax.psum_scatter(jnp.dot(hidden, w_down, preferred_element_type=jnp.float...]
    another operation x0 -> x2, local copies, waits for them, and re-layouts: none -> 5.09 us  [shards(): jnp.stack([arrived_rows] * lax.axis_size('tp'))]
  transfers between devices with their start and end apart: 7 -> 7, of which waited for: 5 -> 4; matrix products, arithmetic and copies ran while one was open for 13% -> 8% of each run, Pallas kernels for 0% -> 0%
where the time goes in v1:
time: 452 us; the launch traced here: 451 us
  waiting for transfers between devices  335 us (74%)
  matrix products  34 us (8%)
  starting transfers between devices  26.8 us (6%)
  blocking collectives  23.4 us (5%)
  between operations  14 us (3%)
  local copies, waits for them, and re-layouts  11.3 us (2%)
  other arithmetic  6.92 us (2%)
    all_to_all x1, waiting for transfers between devices, shards(): lax.all_to_all(jnp.stack([arrived_rows] * lax.axis_size('tp')), 'tp', 0, 0)  244 us
    reduce_scatter x1, waiting for transfers between devices, shards(): lax.psum_scatter(jnp.dot(hidden, w_down, preferred_element_type=jnp.float...  52.8 us
    all_gather x1, waiting for transfers between devices, shards(): lax.all_gather(out_proj, 'tp', axis=0, tiled=True)  36.9 us
    all_to_all x1, blocking collectives, shards(): lax.all_to_all(outgoing.reshape(experts, capacity, width_model), 'ep', sp...  23.4 us
    dot_general x1, matrix products, shards(): jnp.dot(hidden, w_down, preferred_element_type=jnp.float32)  14.9 us
    all_to_all x1, starting transfers between devices, shards(): lax.all_to_all(jnp.stack([arrived_rows] * lax.axis_size('tp')), 'tp', 0, 0)  10.7 us
  transfers between devices with their start and end apart: 7, of which 4 were waited for; matrix products, arithmetic and copies ran while one was open for 8% of the time, Pallas kernels for 0%

profile of v1, /device:TPU:1, one launch (start us, length us, event | category | flops | bytes accessed | tf_op | source)
XLA Modules:
  0.0 451.2 jit_solution(4807373101079785079)
XLA Ops:
  7.2 0.9 copy.25
  8.0 0.1 eq.29
  8.2 0.1 fusion.24
  8.3 0.2 reduce_window_sum.11
  8.4 0.2 select_reduce_fusion
  8.6 0.1 reduce_sum.52
  8.8 0.1 copy.27
  8.9 0.1 fusion.23
  9.0 0.7 convert_element_type.89
  9.7 1.1 fusion.15
  10.8 1.3 convolution_convert_fusion.2
  12.1 0.2 reshape.89
  12.4 23.4 %all_to_all.34 = bf16[16,9,2048]{2,1,0:T(8,128)(2,1)S(1)} all-to-all(bf16[16,9,2048]{2,1,0:T(8,128)(2,1)S(1)} %reshape.89), channel_id=1, replica_groups=mesh['ep'=16,'tp'=16] {'ep'}, dimensions={0} | all-to-all | bytes 1179648 | tf_op jit(solution)/shard_map/all_to_all | solution.py:82
  35.8 0.3 stack_reshape.2
  36.0 4.8 %stack.3 = bf16[16,144,2048]{2,1,0:T(8,128)(2,1)} broadcast(bf16[144,2048]{1,0:T(8,128)(2,1)S(1)} %stack_reshape.2), dimensions={1,2} | broadcast | bytes 10027008 | tf_op jit(solution)/shard_map/stack | solution.py:94
  40.9 10.7 %all-to-all-start.2 = ((bf16[16,144,2048]{2,1,0:T(8,128)(2,1)}), bf16[16,144,2048]{2,1,0:T(8,128)(2,1)}, u32[]{:S(2)}, u32[]{:S(2)}) async-start(bf16[16,144,2048]{2,1,0:T(8,128)(2,1)} %stack.3), calls=%async_computation.2 | async-start | bytes 18874368 | tf_op jit(solution)/shard_map/all_to_all | solution.py:94
  51.5 0.0 all-gather.3.cloned.1.call-start
  51.6 0.2 fusion.2
  51.8 1.0 fusion.4
  52.8 0.0 reduce-scatter.2.cloned.1.call-start
  52.9 243.8 %all-to-all-done.2 = bf16[16,144,2048]{2,1,0:T(8,128)(2,1)} async-done(((bf16[16,144,2048]{2,1,0:T(8,128)(2,1)}), bf16[16,144,2048]{2,1,0:T(8,128)(2,1)}, u32[]{:S(2)}, u32[]{:S(2)}) %all-to-all-start.2) | async-done | bytes 9437216 | tf_op jit(solution)/shard_map/all_to_all | solution.py:94
  296.7 7.7 %fusion.8 = f32[2304,256]{1,0:T(8,128)} fusion(bf16[2304,2048]{1,0:T(8,128)(2,1)} %bitcast.5, bf16[1,2048,256]{2,1,0:T(8,128)(2,1)S(1)} %copy-done.5), kind=kOutput, calls=%fused_computation.15 | convolution fusion | flops 2415919104 | bytes 12845056 | tf_op jit(solution)/shard_map/dot_general | solution.py:96
  304.4 14.9 %convolution_convert_fusion = bf16[2304,2048]{1,0:T(8,128)(2,1)} fusion(bf16[2304,2048]{1,0:T(8,128)(2,1)} %bitcast.5, f32[2304,256]{1,0:T(8,128)} %fusion.8, bf16[1,256,2048]{2,1,0:T(8,128)(2,1)S(1)} %copy-done, bf16[1,2048,256]{2,1,0:T(8,128)(2,1)} %param.26), kind=kOutput, calls=%fused_computation.1 | convolution fusion | flops 4840095744 | bytes 23330816 | tf_op jit(solution)/shard_map/dot_general | solution.py:100
  319.3 0.0 reduce-scatter.2.cloned.1.call-update
  319.4 0.0 all-gather.5.cloned.1.call-start
  319.4 0.7 all-gather.5.cloned.1.call-update
  320.1 0.0 all-gather.3.cloned.1.call-done
  320.2 0.1 copy-done.6
  320.3 0.1 copy-done.7
  320.4 0.1 copy-done.8
  320.4 6.3 %convolution_convert_fusion.1 = bf16[2048,192]{0,1:T(8,128)(2,1)S(1)} fusion(bf16[2048,2048]{1,0:T(8,128)(2,1)} %all-gather.3.cloned.1.call-done, bf16[2048,64]{0,1:T(8,128)(2,1)S(1)} %copy-done.6, bf16[2048,64]{0,1:T(8,128)(2,1)S(1)} %copy-done.7, bf16[2048,64]{0,1:T(8,128)(2,1)S(1)} %copy-done.8), kind=kOutput, calls=%fused_computation.4 | convolution fusion | flops 1613365248 | bytes 9961472 | tf_op jit(solution)/shard_map/dot_general | solution.py:39
  326.7 0.1 multiply_convert_fusion.1
  326.8 0.1 slice.41
  326.9 2.4 collective-permute-start
  329.3 0.7 collective-permute-done
  329.9 1.0 copy_bitcast_fusion
  330.9 6.5 %all-to-all-start = ((bf16[16,128,64]{1,2,0:T(8,128)(2,1)}), bf16[16,128,64]{1,2,0:T(8,128)(2,1)S(1)}, u32[]{:S(2)}, u32[]{:S(2)}) async-start(bf16[16,128,64]{1,2,0:T(8,128)(2,1)} %copy_bitcast_fusion), calls=%async_computation | async-start | bytes 524288 | tf_op jit(solution)/shard_map/all_to_all | solution.py:60
  337.4 0.1 mul.138
  337.6 52.8 %reduce-scatter.2.cloned.1.call-done = bf16[144,2048]{1,0:T(8,128)(2,1)} async-done(((bf16[2304,2048]{1,0:T(8,128)(2,1)}), bf16[144,2048]{1,0:T(8,128)(2,1)}) %reduce-scatter.2.cloned.1.call-update) | async-done | bytes 589840 | tf_op jit(solution)/shard_map/reduce_scatter | solution.py:99
  390.4 2.3 reshape.91
  392.7 7.2 %all-to-all-start.3 = ((bf16[16,9,2048]{2,1,0:T(8,128)(2,1)}), bf16[16,9,2048]{2,1,0:T(8,128)(2,1)S(1)}, u32[]{:S(2)}, u32[]{:S(2)}) async-start(bf16[16,9,2048]{2,1,0:T(8,128)(2,1)} %reshape.91), calls=%async_computation.4 | async-start | bytes 2097152 | tf_op jit(solution)/shard_map/all_to_all | solution.py:105
  399.9 0.1 copy.24
  400.0 36.9 %all-gather.5.cloned.1.call-done = bf16[1024,2048]{1,0:T(8,128)(2,1)} async-done(((bf16[64,2048]{1,0:T(8,128)(2,1)}), bf16[1024,2048]{1,0:T(8,128)(2,1)}) %all-gather.5.cloned.1.call-update) | async-done | bytes 4194320 | tf_op jit(solution)/shard_map/all_gather | solution.py:63
  436.9 3.7 convolution_convert_fusion.3
  440.6 0.3 reshape.92
  440.9 0.9 gather_fusion
  441.8 0.7 reshape.93
  442.5 2.3 multiply_reduce_fusion
  (29 shorter events, 0.2 us)
Async XLA Ops:
  7.2 297.2 %copy-start = (bf16[1,256,2048]{2,1,0:T(8,128)(2,1)S(1)}, bf16[1,256,2048]{2,1,0:T(8,128)(2,1)}, u32[]{:S(2)}) copy-start(bf16[1,256,2048]{2,1,0:T(8,128)(2,1)} %param.27) | copy-start | bytes 3145732
  40.9 10.7 %copy-start.3 = (bf16[2048]{0:T(1024)(128)(2,1)S(1)}, bf16[2048]{0:T(1024)(128)(2,1)}, u32[]{:S(2)}) copy-start(bf16[2048]{0:T(1024)(128)(2,1)} %param.15) | copy-start | bytes 12292
  40.9 10.7 %copy-start.1 = (bf16[128,2048]{1,0:T(8,128)(2,1)S(1)}, bf16[128,2048]{1,0:T(8,128)(2,1)}, u32[]{:S(2)}) copy-start(bf16[128,2048]{1,0:T(8,128)(2,1)} %param.14) | copy-start | bytes 1572868
  40.9 255.8 %copy-start.5 = (bf16[1,2048,256]{2,1,0:T(8,128)(2,1)S(1)}, bf16[1,2048,256]{2,1,0:T(8,128)(2,1)}, u32[]{:S(2)}) copy-start(bf16[1,2048,256]{2,1,0:T(8,128)(2,1)} %param.25) | copy-start | bytes 3145732
  40.9 255.8 %all-to-all-start.2 = ((bf16[16,144,2048]{2,1,0:T(8,128)(2,1)}), bf16[16,144,2048]{2,1,0:T(8,128)(2,1)}, u32[]{:S(2)}, u32[]{:S(2)}) async-start(bf16[16,144,2048]{2,1,0:T(8,128)(2,1)} %stack.3), calls=%async_computation.2 | async-start | bytes 18874368 | tf_op jit(solution)/shard_map/all_to_all | solution.py:94
  51.5 268.6 %all-gather.3.cloned.1.call-start = ((), (), s32[]{:S(2)}) async-start(), calls=%async_computation.5 | async-start | bytes 8912896 | tf_op jit(solution)/shard_map/all_gather | solution.py:40
  52.8 337.6 %reduce-scatter.2.cloned.1.call-start = ((), (), s32[]{:S(2)}) async-start(), calls=%async_computation.7 | async-start | bytes 10027008 | tf_op jit(solution)/shard_map/reduce_scatter | solution.py:99
  319.3 0.8 copy-start.4
  319.3 1.0 copy-start.6
  319.3 1.0 copy-start.7
  319.3 1.1 copy-start.8
  319.4 117.5 %all-gather.5.cloned.1.call-start = ((), (), s32[]{:S(2)}) async-start(), calls=%async_computation.6 | async-start | bytes 4456448 | tf_op jit(solution)/shard_map/all_gather | solution.py:63
  320.1 17.4 %copy-start.2 = (f32[64,2]{0,1:T(2,128)S(1)}, f32[64,2]{0,1:T(2,128)}, u32[]{:S(2)}) copy-start(f32[64,2]{0,1:T(2,128)} %param.24) | copy-start | bytes 1540
  326.9 3.0 collective-permute-start
  330.9 61.8 %all-to-all-start = ((bf16[16,128,64]{1,2,0:T(8,128)(2,1)}), bf16[16,128,64]{1,2,0:T(8,128)(2,1)S(1)}, u32[]{:S(2)}, u32[]{:S(2)}) async-start(bf16[16,128,64]{1,2,0:T(8,128)(2,1)} %copy_bitcast_fusion), calls=%async_computation | async-start | bytes 524288 | tf_op jit(solution)/shard_map/all_to_all | solution.py:60
  392.7 47.9 %all-to-all-start.3 = ((bf16[16,9,2048]{2,1,0:T(8,128)(2,1)}), bf16[16,9,2048]{2,1,0:T(8,128)(2,1)S(1)}, u32[]{:S(2)}, u32[]{:S(2)}) async-start(bf16[16,9,2048]{2,1,0:T(8,128)(2,1)} %reshape.91), calls=%async_computation.4 | async-start | bytes 2097152 | tf_op jit(solution)/shard_map/all_to_all | solution.py:105
Sparse Core Ops, SparseCore 0:
  54.8 163.0 all-gather.2
  319.5 70.8 reduce-scatter.1
  392.2 44.5 all-gather.4
